TPU v7x, 32 devices: a whole 2x2x4 slice. The times are simulated.
32 devices in a mesh: sp: 4 (over y, x), tp: 8 (over z, core).
Axes of the slice: x: 2, y: 2, z: 4, core: 2. Of those that a mesh axis runs over, the one named last changes fastest.
Arguments:
- tokens: bfloat16 [8, 3072, 2048], P(None, ('sp', 'tp')), may hold values from -13 to 13
- in_gain: float32 [2048], replicated, may hold values from 0.1 to 1.9
- w_key: bfloat16 [2048, 512], P('tp'), may hold values from -0.125 to 0.125
- w_value: bfloat16 [2048, 512], P('tp'), may hold values from -0.125 to 0.125
- k_gain: float32 [128], replicated, may hold values from 0.1 to 1.9
- new_query: bfloat16 [8, 1024], replicated, may hold values from -6 to 6
- q_gain: float32 [128], replicated, may hold values from 0.1 to 1.9
- stick_bias: float32 [8], replicated, may hold values from -13 to -3
Outputs:
- key_cache: bfloat16 [32, 3072, 128], P('tp', 'sp')
- value_cache: bfloat16 [32, 3072, 128], P('tp', 'sp')
- read_out: float32 [32, 256], P('tp')
All inputs are finite; a program needn't handle non-finite values.
Results may differ from a plain program's by a relative error of at most 0.005.
Values may be sent and summed in bfloat16 or wider, within the bound.
A program may use at most 64 MiB of HBM per device.

v0:
```python
import jax
import jax.numpy as jnp
from jax import lax
from jax.sharding import PartitionSpec as P

NORM_EPS = 1e-06


def entering(value, axis, join, neutral):
    count, mine = (lax.axis_size(axis), lax.axis_index(axis))
    pieces = lax.all_gather(value, axis)
    pieces = pieces[::-1]
    mine = count - 1 - mine
    so_far = jnp.full_like(value, 0) + jnp.asarray(neutral, value.dtype)

    def turn(position, so_far):
        longer = join(so_far, pieces[position])
        return jnp.where(position < mine, longer, so_far)

    return lax.fori_loop(0, count - 1, turn, so_far)


def root_norm(values, scaling):
    inverse = lax.rsqrt(jnp.mean(values * values, axis=-1, keepdims=True) + NORM_EPS)
    return values * inverse * scaling


def add_later(earlier, later_part):
    return earlier + later_part


def shards(tokens, in_gain, w_key, w_value, k_gain, new_query, q_gain, stick_bias):
    seq_count, tok_seq, model_width = tokens.shape
    row_count = seq_count * tok_seq
    head_dim = k_gain.shape[0]
    kv_width = w_key.shape[1]
    kv_heads = kv_width // head_dim
    per_group = stick_bias.shape[0] // kv_heads
    inv_root = head_dim ** (-0.5)
    normed = root_norm(tokens.reshape(row_count, model_width).astype(jnp.float32), in_gain).astype(
        jnp.bfloat16
    )
    key_raw = jnp.dot(
        normed, lax.all_gather(w_key, "tp", axis=0, tiled=True), preferred_element_type=jnp.float32
    )
    value_raw = jnp.dot(
        normed,
        lax.all_gather(w_value, "tp", axis=0, tiled=True),
        preferred_element_type=jnp.float32,
    )
    key_rows = root_norm(key_raw.reshape(seq_count, tok_seq, kv_heads, head_dim), k_gain).astype(
        jnp.bfloat16
    )
    value_rows = value_raw.astype(jnp.bfloat16).reshape(seq_count, tok_seq, kv_heads, head_dim)
    query_rows = root_norm(
        new_query.astype(jnp.float32).reshape(seq_count, kv_heads, per_group, head_dim), q_gain
    ).astype(jnp.bfloat16)
    bias_rows = stick_bias.reshape(kv_heads, per_group)
    key_block = key_rows.transpose(2, 0, 1, 3).reshape(kv_heads * seq_count, tok_seq, head_dim)
    value_block = value_rows.transpose(2, 0, 1, 3).reshape(kv_heads * seq_count, tok_seq, head_dim)
    key_cache, value_cache = (
        lax.all_to_all(key_block, "tp", split_axis=0, concat_axis=1, tiled=True),
        lax.all_to_all(value_block, "tp", split_axis=0, concat_axis=1, tiled=True),
    )
    group_rows = key_cache.shape[0]
    row_start = lax.axis_index("tp") * group_rows
    query_flat = query_rows.transpose(1, 0, 2, 3).reshape(kv_heads * seq_count, per_group, head_dim)
    query_group = lax.dynamic_slice_in_dim(query_flat, row_start, group_rows, 0)
    bias_group = lax.dynamic_slice_in_dim(
        jnp.repeat(bias_rows, seq_count, axis=0), row_start, group_rows, 0
    )
    scores = (
        jnp.einsum("rqe,rpe->rqp", query_group, key_cache, preferred_element_type=jnp.float32)
        * inv_root
        + bias_group[:, :, None]
    )
    log_keep = jax.nn.log_sigmoid(-scores)
    log_total = jnp.sum(log_keep, axis=2)
    log_later = entering(log_total, "sp", add_later, jnp.zeros_like(log_total))
    log_after = log_later[:, :, None] + lax.cumsum(log_keep, axis=2, reverse=True) - log_keep
    weights = jnp.exp(jax.nn.log_sigmoid(scores) + log_after).astype(jnp.bfloat16)
    partial_value = jnp.einsum(
        "rqp,rpe->rqe", weights, value_cache, preferred_element_type=jnp.float32
    )
    read_out = lax.psum(partial_value.reshape(group_rows, per_group * head_dim), "sp")
    return (key_cache, value_cache, read_out)


def solution(mesh):
    return jax.shard_map(
        shards,
        mesh=mesh,
        in_specs=(
            P(None, ("sp", "tp"), None),
            P(),
            P("tp", None),
            P("tp", None),
            P(),
            P(),
            P(),
            P(),
        ),
        out_specs=(P("tp", "sp", None), P("tp", "sp", None), P("tp", None)),
        check_vma=False,
    )
```

profile of v0, /device:TPU:0, one launch (start us, length us, event | category | flops | bytes accessed | tf_op | source)
XLA Modules:
  0.0 152.8 jit_solution(754454216870230095)
XLA Ops:
  7.2 0.7 all-gather.5.cloned.1.call-update
  7.9 0.7 all-gather.7.cloned.1.call-update
  8.7 2.7 %multiply_reduce_fusion = f32[8,96]{1,0:T(8,128)S(1)} fusion(bf16[8,96,2048]{2,1,0:T(8,128)(2,1)} %param.10), kind=kLoop, calls=%fused_computation.5 | loop fusion | flops 4717824 | bytes 3148800 | tf_op jit(solution)/shard_map/reduce_sum | solution.py:24
  11.4 30.1 %all-gather.5.cloned.1.call-done = bf16[2048,512]{1,0:T(8,128)(2,1)} async-done(((bf16[256,512]{1,0:T(8,128)(2,1)}), bf16[2048,512]{1,0:T(8,128)(2,1)}) %all-gather.5.cloned.1.call-update) | async-done | bytes 2097168 | tf_op jit(solution)/shard_map/all_gather | solution.py:44
  41.5 3.9 %copy.25 = bf16[512,2048]{1,0:T(8,128)(2,1)} copy(bf16[512,2048]{0,1:T(8,128)(2,1)} %bitcast.63) | data formatting | bytes 4194304 | tf_op jit(solution)/shard_map/dot_general | solution.py:43
  45.4 3.9 %multiply_reduce_fusion.1 = (f32[8,96,4]{1,2,0:T(4,128)S(1)}, f32[8,96,4,128]{3,1,2,0:T(8,128)S(1)}) fusion(bf16[4,128,2048,1]{2,1,0,3:T(8,128)(2,1)} %bitcast.64, f32[2048]{0:T(1024)S(1)} %copy-done.4, f32[8,96]{1,0:T(8,128)S(1)} %add_rsqrt_fusion.1, bf16[8,96,2048]{2,1,0:T(8,128)(2,1)S(1)} %copy-done), kind=kOutput, calls=%fused_computation.14 | convolution fusion | flops 1617687552 | bytes 6839296 | tf_op jit(solution)/shard_map/dot_general | solution.py:43
  49.3 0.5 fusion.9
  49.8 0.9 copy.26
  50.7 4.2 %all-to-all-start = ((bf16[32,96,128]{2,1,0:T(8,128)(2,1)}), bf16[32,96,128]{2,1,0:T(8,128)(2,1)}, u32[]{:S(2)}, u32[]{:S(2)}) async-start(bf16[32,96,128]{2,1,0:T(8,128)(2,1)} %bitcast.62), calls=%async_computation | async-start | bytes 1572864 | tf_op jit(solution)/shard_map/all_to_all | solution.py:62
  55.0 2.5 %fusion.1 = bf16[768,2048]{1,0:T(8,128)(2,1)} fusion(f32[2048]{0:T(1024)S(1)} %copy-done.4, f32[768]{0:T(1024)S(1)} %rsqrt.35, bf16[8,96,2048]{2,1,0:T(8,128)(2,1)S(1)} %copy-done), kind=kLoop, calls=%fused_computation.3 | loop fusion | flops 6291456 | bytes 6302720 | tf_op jit(solution)/shard_map/convert_element_type | solution.py:40
  57.5 28.8 %all-gather.7.cloned.1.call-done = bf16[2048,512]{1,0:T(8,128)(2,1)} async-done(((bf16[256,512]{1,0:T(8,128)(2,1)}), bf16[2048,512]{1,0:T(8,128)(2,1)}) %all-gather.7.cloned.1.call-update) | async-done | bytes 2097168 | tf_op jit(solution)/shard_map/all_gather | solution.py:48
  86.3 4.3 %convolution_convert_fusion = bf16[768,512]{1,0:T(8,128)(2,1)S(1)} fusion(bf16[768,2048]{1,0:T(8,128)(2,1)} %fusion.1, bf16[2048,512]{1,0:T(8,128)(2,1)} %all-gather.7.cloned.1.call-done), kind=kOutput, calls=%fused_computation.15 | convolution fusion | flops 1611005952 | bytes 6029312 | tf_op jit(solution)/shard_map/dot_general | solution.py:46
  90.7 0.2 reshape.106
  90.8 1.0 copy.28
  91.9 3.5 %all-to-all-start.1 = ((bf16[32,96,128]{2,1,0:T(8,128)(2,1)}), bf16[32,96,128]{2,1,0:T(8,128)(2,1)S(1)}, u32[]{:S(2)}, u32[]{:S(2)}) async-start(bf16[32,96,128]{2,1,0:T(8,128)(2,1)} %bitcast.13), calls=%async_computation.1 | async-start | bytes 1572864 | tf_op jit(solution)/shard_map/all_to_all | solution.py:63
  95.5 0.1 copy.31
  95.7 0.1 reshape.112
  95.8 0.1 copy.32
  95.9 0.1 fusion.11
  96.2 1.2 copy.27
  97.4 18.9 %all-to-all-done.1 = bf16[32,96,128]{2,1,0:T(8,128)(2,1)S(1)} async-done(((bf16[32,96,128]{2,1,0:T(8,128)(2,1)}), bf16[32,96,128]{2,1,0:T(8,128)(2,1)S(1)}, u32[]{:S(2)}, u32[]{:S(2)}) %all-to-all-start.1) | async-done | bytes 786464 | tf_op jit(solution)/shard_map/all_to_all | solution.py:63
  116.4 0.3 fusion.24
  116.7 0.2 fusion.29
  116.9 9.9 %reduce-window.6 = f32[4,2,6,128]{3,2,1,0:T(8,128)S(1)} reduce-window(f32[4,2,6,128]{3,2,1,0:T(8,128)S(1)} %reshape.113, f32[]{:T(128)} %constant.50.clone.1), window={size=1x1x1x128 pad=0_0x0_0x0_0x0_127}, to_apply=%region_6.7 | reduce-window | flops 780288 | bytes 49156 | tf_op jit(solution)/shard_map/reduce-window
  126.8 0.1 slice_reduce_fusion
  126.9 0.7 reduce-window.9
  127.8 0.1 copy.33
  127.9 8.0 %all-gather.1 = f32[4,4,2]{1,2,0:T(2,128)S(1)} all-gather(f32[1,4,2]{1,2,0:T(2,128)S(1)} %bitcast.71), channel_id=2, replica_groups=mesh['sp'=4,'tp'=8] {'sp'}, dimensions={0}, use_global_device_ids=true | all-gather | bytes 160 | tf_op jit(solution)/shard_map/all_gather | solution.py:11
  135.9 0.1 while.14
  136.0 0.1 copy.34
  136.1 0.3 convolution_bitcast_fusion
  136.4 9.5 %psum.7 = f32[4,256]{1,0:T(4,128)} all-reduce(f32[4,256]{1,0:T(4,128)S(1)} %bitcast.70), channel_id=1, replica_groups=mesh['sp'=4,'tp'=8] {'sp'}, use_global_device_ids=true, to_apply=%region_8.9 | all-reduce | flops 1024 | bytes 8192 | tf_op jit(solution)/shard_map/psum | solution.py:85
  (41 shorter events, 0.9 us)
Async XLA Ops:
  7.2 34.3 %all-gather.5.cloned.1.call-start = ((), (), s32[]{:S(2)}) async-start(), calls=%async_computation.2 | async-start | bytes 2359296 | tf_op jit(solution)/shard_map/all_gather | solution.py:44
  7.9 78.4 %all-gather.7.cloned.1.call-start = ((), (), s32[]{:S(2)}) async-start(), calls=%async_computation.3 | async-start | bytes 2359296 | tf_op jit(solution)/shard_map/all_gather | solution.py:48
  8.6 36.8 %copy-start = (bf16[8,96,2048]{2,1,0:T(8,128)(2,1)S(1)}, bf16[8,96,2048]{2,1,0:T(8,128)(2,1)}, u32[]{:S(2)}) copy-start(bf16[8,96,2048]{2,1,0:T(8,128)(2,1)} %param.10) | copy-start | bytes 9437188
  8.7 36.8 %copy-start.4 = (f32[2048]{0:T(1024)S(1)}, f32[2048]{0:T(1024)}, u32[]{:S(2)}) copy-start(f32[2048]{0:T(1024)} %param.11) | copy-start | bytes 24580
  45.4 3.9 %copy-start.7 = (f32[128]{0:T(128)S(1)}, f32[128]{0:T(128)}, u32[]{:S(2)}) copy-start(f32[128]{0:T(128)} %param.14) | copy-start | bytes 1540
  50.7 41.1 %all-to-all-start = ((bf16[32,96,128]{2,1,0:T(8,128)(2,1)}), bf16[32,96,128]{2,1,0:T(8,128)(2,1)}, u32[]{:S(2)}, u32[]{:S(2)}) async-start(bf16[32,96,128]{2,1,0:T(8,128)(2,1)} %bitcast.62), calls=%async_computation | async-start | bytes 1572864 | tf_op jit(solution)/shard_map/all_to_all | solution.py:62
  90.6 4.8 %copy-start.6 = (f32[8]{0:T(128)S(1)}, f32[8]{0:T(128)}, u32[]{:S(2)}) copy-start(f32[8]{0:T(128)} %param.17) | copy-start | bytes 100
  90.6 5.3 %copy-start.3 = (bf16[8,1024]{1,0:T(8,128)(2,1)S(1)}, bf16[8,1024]{1,0:T(8,128)(2,1)}, u32[]{:S(2)}) copy-start(bf16[8,1024]{1,0:T(8,128)(2,1)} %param.15) | copy-start | bytes 49156
  90.6 5.4 %copy-start.5 = (f32[128]{0:T(128)S(1)}, f32[128]{0:T(128)}, u32[]{:S(2)}) copy-start(f32[128]{0:T(128)} %param.16) | copy-start | bytes 1540
  91.9 24.4 %all-to-all-start.1 = ((bf16[32,96,128]{2,1,0:T(8,128)(2,1)}), bf16[32,96,128]{2,1,0:T(8,128)(2,1)S(1)}, u32[]{:S(2)}, u32[]{:S(2)}) async-start(bf16[32,96,128]{2,1,0:T(8,128)(2,1)} %bitcast.13), calls=%async_computation.1 | async-start | bytes 1572864 | tf_op jit(solution)/shard_map/all_to_all | solution.py:63
  97.4 48.6 %copy-start.1 = (bf16[4,8,96,128]{3,2,1,0:T(8,128)(2,1)}, bf16[4,8,96,128]{3,2,1,0:T(8,128)(2,1)S(1)}, u32[]{:S(2)}) copy-start(bf16[4,8,96,128]{3,2,1,0:T(8,128)(2,1)S(1)} %copy.27) | copy-start | bytes 2359300
  116.3 29.6 %copy-start.2 = (bf16[4,8,96,128]{3,2,1,0:T(8,128)(2,1)}, bf16[4,8,96,128]{3,2,1,0:T(8,128)(2,1)S(1)}, u32[]{:S(2)}) copy-start(bf16[4,8,96,128]{3,2,1,0:T(8,128)(2,1)S(1)} %copy.29) | copy-start | bytes 2359300
Sparse Core Ops, SparseCore 0:
  9.6 31.8 all-gather.4
  43.1 43.1 all-gather.6
where the time goes:
time: 153 us
  waiting for transfers between devices  79.1 us (52%)
  blocking collectives  17.6 us (12%)
  other arithmetic  16.8 us (11%)
  between operations  14.3 us (9%)
  matrix products  8.78 us (6%)
  local copies, waits for them, and re-layouts  8.35 us (5%)
  starting transfers between devices  7.84 us (5%)
    all_gather x1, waiting for transfers between devices, shards(): lax.all_gather(w_key, 'tp', axis=0, tiled=True)  30.1 us
    all_gather x1, waiting for transfers between devices, shards(): lax.all_gather(w_value, 'tp', axis=0, tiled=True)  28.8 us
    all_to_all x1, waiting for transfers between devices, shards(): lax.all_to_all(value_block, 'tp', split_axis=0, concat_axis=1, tiled=True)  18.9 us
    another operation x2, other arithmetic  10.6 us
    psum x1, blocking collectives, shards(): lax.psum(partial_value.reshape(group_rows, per_group * head_dim), 'sp')  9.53 us
    all_gather x1, blocking collectives, entering(): pieces = lax.all_gather(value, axis)  8.04 us
    dot_general x1, matrix products, shards(): jnp.dot(normed, lax.all_gather(w_value, 'tp', axis=0, tiled=True), prefer...  4.32 us
    all_to_all x1, starting transfers between devices, shards(): lax.all_to_all(key_block, 'tp', split_axis=0, concat_axis=1, tiled=True)  4.21 us
  transfers between devices with their start and end apart: 4, of which 3 were waited for; matrix products, arithmetic and copies ran while one was open for 14% of the time, Pallas kernels for 0%

commit v1 on v0

v1 whole, which is shorter than its diff:
```python
import functools

import jax
import jax.numpy as jnp
from jax import lax
from jax.experimental import pallas as pl
from jax.experimental.pallas import tpu as pltpu
from jax.sharding import PartitionSpec as P

NORM_EPS = 1e-06
MESH = pl.DeviceIdType.MESH
CORES = 2
SUBLANES = 16


def root_norm(values, scaling):
    inverse = lax.rsqrt(jnp.mean(values * values, axis=-1, keepdims=True) + NORM_EPS)
    return values * inverse * scaling


def remote(src, dst, send, recv, sp, tp):
    return pltpu.make_async_remote_copy(
        src_ref=src, dst_ref=dst, send_sem=send, recv_sem=recv, device_id=(sp, tp), device_id_type=MESH
    )


def kernel(
    dims,
    tok_hbm, gain_ref, wk_hbm, wv_hbm, kgain_ref, query_ref, bias_ref,
    kc_hbm, vc_hbm, read_ref,
    tok, normed, wbuf, kbuf, vbuf, krecv, vrecv, parts,
    tok_sem, own_sem, p1_send, p1_recv, p2_send, p2_recv, p3_send, p3_recv,
    a_send, a_recv, mine_sem, out_sem, f_send, f_recv,
):
    nsp, ntp, heads, q, group_rows, per_group = dims
    sp, tp = lax.axis_index("sp"), lax.axis_index("tp")
    nz = ntp // CORES
    z, c = tp // CORES, tp % CORES
    partner = z * CORES + (1 - c)
    base, i = (sp // q) * q, sp % q
    seqs, tok_seq, width = tok.shape
    rows = wk_hbm.shape[0]
    part = rows // q
    hd = kc_hbm.shape[2]
    span = ntp * tok_seq
    tp_head = ntp // heads
    half = heads // 2

    def head_at(zc, j):
        home = (zc * CORES) // tp_head
        side = (home // half + (1 if j < half else 0)) % 2
        return side * half + (home % half + (half - 1 - j % half)) % half

    fetch = pltpu.make_async_copy(tok_hbm, tok, tok_sem)
    own = []
    for j in range(heads):
        h = head_at(z, j)
        cols = pl.ds(pl.multiple_of(h * hd, hd), hd)
        for n, w in enumerate((wk_hbm, wv_hbm)):
            copy = pltpu.make_async_copy(
                w.at[:, cols], wbuf.at[h, z, c, :, pl.ds(n * hd, hd)], own_sem.at[j, n]
            )
            copy.start()
            own.append(copy)
    fetch.start()

    barrier = pltpu.get_barrier_semaphore()
    for d in range(1, ntp):
        pl.semaphore_signal(barrier, inc=1, device_id=(sp, (tp + d) % ntp), device_id_type=MESH)
    for d in range(1, nsp):
        pl.semaphore_signal(barrier, inc=1, device_id=((sp + d) % nsp, tp), device_id_type=MESH)
    for copy in own:
        copy.wait()
    pl.semaphore_wait(barrier, ntp + nsp - 2)

    mine = pl.ds(pl.multiple_of(i * part, part), part)
    sends = []

    for j in range(heads):
        for d in range(1, nz):
            zt = (z + d) % nz
            h = head_at(zt, j)
            block = wbuf.at[h, z, c, mine]
            copy = remote(block, block, p1_send.at[j, d], p1_recv.at[j, z], sp, zt * CORES + c)
            copy.start()
            sends.append(copy)

    fetch.wait()
    step_rows = SUBLANES
    per_seq = tok_seq // step_rows

    def norm_rows(n, carry):
        s, at = n // per_seq, pl.ds(pl.multiple_of((n % per_seq) * step_rows, step_rows), step_rows)
        values = tok[s, at].astype(jnp.float32)
        normed[s, at] = root_norm(values, gain_ref[...]).astype(jnp.bfloat16)
        return carry

    lax.fori_loop(0, seqs * per_seq, norm_rows, 0)

    def spread(j):
        h = head_at(z, j)
        for d in range(1, nz):
            zs = (z + nz - d) % nz
            block = wbuf.at[h, zs, c, mine]
            remote(block, block, p1_send.at[j, d], p1_recv.at[j, zs], sp, zs * CORES + c).wait_recv()
            for e in range(1, q):
                copy = remote(
                    block, block, p2_send.at[j, e, d], p2_recv.at[j, i, zs], base + (i + e) % q, tp
                )
                copy.start()
                sends.append(copy)

    def share(j):
        h = head_at(z, j)
        for d in range(1, nz):
            zs = (z + nz - d) % nz
            for e in range(1, q):
                source = (i + e) % q
                block = wbuf.at[h, zs, c, pl.ds(pl.multiple_of(source * part, part), part)]
                remote(
                    block, block, p2_send.at[j, e, d], p2_recv.at[j, source, zs], base + source, tp
                ).wait_recv()
        block = wbuf.at[h, :, c]
        copy = remote(block, block, p3_send.at[j], p3_recv.at[j], sp, partner)
        copy.start()
        sends.append(copy)

    tile = seqs // 2

    def project(j):
        h = head_at(z, j)
        block = wbuf.at[h, :, 1 - c]
        remote(block, block, p3_send.at[j], p3_recv.at[j], sp, partner).wait_recv()

        def rows_of(n, carry):
            at = pl.ds(n * tile, tile)
            both = jnp.dot(
                normed[at].reshape(tile * tok_seq, width),
                wbuf[h].reshape(width, 2 * hd),
                preferred_element_type=jnp.float32,
            )
            key = root_norm(both[:, :hd], kgain_ref[...])
            kbuf[h, at] = key.astype(jnp.bfloat16).reshape(tile, tok_seq, hd)
            vbuf[h, at] = both[:, hd:].astype(jnp.bfloat16).reshape(tile, tok_seq, hd)
            return carry

        lax.fori_loop(0, seqs // tile, rows_of, 0)

    here = pl.ds(pl.multiple_of(tp * tok_seq, tok_seq), tok_seq)

    def deliver(j):
        h = head_at(z, j)
        for u in range(tp_head):
            target = h * tp_head + u
            at = pl.ds(u * group_rows, group_rows)

            def send(target=target, at=at):
                for n, (src, dst) in enumerate(((kbuf, krecv), (vbuf, vrecv))):
                    remote(
                        src.at[h, at], dst.at[:, here], a_send.at[n, target], a_recv.at[n, tp], sp, target
                    ).start()

            if j < heads - 1:
                send()
            else:

                @pl.when(target != tp)
                def _():
                    send()

                @pl.when(target == tp)
                def _():
                    for n, (src, dst) in enumerate(((kbuf, krecv), (vbuf, vrecv))):
                        pltpu.make_async_copy(src.at[h, at], dst.at[:, here], mine_sem.at[n]).start()

    spread(0)
    for j in range(heads):
        if j + 1 < heads:
            spread(j + 1)
        share(j)
        project(j)
        deliver(j)

    first = pl.ds(0, group_rows)
    for n, (src, dst) in enumerate(((kbuf, krecv), (vbuf, vrecv))):
        pltpu.make_async_copy(src.at[0, first], dst.at[:, here], mine_sem.at[n]).wait()
    for d in range(1, ntp):
        source = (tp + d) % ntp
        at = pl.ds(pl.multiple_of(source * tok_seq, tok_seq), tok_seq)
        for n, (src, dst) in enumerate(((kbuf, krecv), (vbuf, vrecv))):
            remote(
                src.at[0, first], dst.at[:, at], a_send.at[n, source], a_recv.at[n, source], sp, source
            ).wait_recv()
    outs = (
        pltpu.make_async_copy(krecv, kc_hbm, out_sem.at[0]),
        pltpu.make_async_copy(vrecv, vc_hbm, out_sem.at[1]),
    )
    for copy in outs:
        copy.start()

    lines = query_ref.shape[0]
    line = lax.broadcasted_iota(jnp.int32, (lines, 1), 0) // per_group
    raw = jnp.zeros((lines, span), jnp.float32)
    for r in range(group_rows):
        dots = lax.dot_general(
            query_ref[...], krecv[r], (((1,), (1,)), ((), ())), preferred_element_type=jnp.float32
        )
        raw = jnp.where(line == r, dots, raw)
    scores = raw * hd ** (-0.5) + bias_ref[...][:, :1]
    soft = jnp.log1p(jnp.exp(-jnp.abs(scores)))
    keep = -jnp.maximum(scores, 0.0) - soft
    take = jnp.minimum(scores, 0.0) - soft
    place = lax.broadcasted_iota(jnp.int32, (lines, span), 1)
    total = keep
    reach = 1
    while reach < span:
        moved = pltpu.roll(total, span - reach, 1)
        total = total + jnp.where(place < span - reach, moved, 0.0)
        reach *= 2
    weights = jnp.exp(take + (total - keep)).astype(jnp.bfloat16)
    value = jnp.zeros((lines, hd), jnp.float32)
    for r in range(group_rows):
        dots = jnp.dot(weights, vrecv[r], preferred_element_type=jnp.float32)
        value = jnp.where(line == r, dots, value)
    parts[sp, :, :hd] = value
    parts[sp, :, hd:] = jnp.broadcast_to(total[:, :1], (lines, hd))
    for d in range(1, nsp):
        copy = remote(
            parts.at[sp], parts.at[sp], f_send.at[d], f_recv.at[sp], (sp + d) % nsp, tp
        )
        copy.start()
        sends.append(copy)
    for d in range(1, nsp):
        source = (sp + d) % nsp
        remote(parts.at[source], parts.at[source], f_send.at[d], f_recv.at[source], source, tp).wait_recv()
    result = jnp.zeros((lines, hd), jnp.float32)
    later = jnp.zeros((lines, hd), jnp.float32)
    for n in reversed(range(nsp)):
        result = result + jnp.exp(later) * parts[n, :, :hd]
        later = later + parts[n, :, hd:]
    read_ref[...] = result

    for copy in sends:
        copy.wait_send()
    for d in range(1, ntp):
        target = (tp + d) % ntp
        for n, (src, dst) in enumerate(((kbuf, krecv), (vbuf, vrecv))):
            remote(
                src.at[0, first], dst.at[:, here], a_send.at[n, target], a_recv.at[n, tp], sp, target
            ).wait_send()
    for copy in outs:
        copy.wait()


def shards(sizes, tokens, in_gain, w_key, w_value, k_gain, new_query, q_gain, stick_bias):
    nsp, ntp = sizes
    seqs, tok_seq, width = tokens.shape
    rows, kv_width = w_key.shape
    hd = k_gain.shape[0]
    heads = kv_width // hd
    per_group = stick_bias.shape[0] // heads
    group_rows = heads * seqs // ntp
    used = group_rows * per_group
    lines = -(-used // 8) * 8
    nz = ntp // CORES
    q = min(nsp, rows // SUBLANES)
    query = root_norm(
        new_query.astype(jnp.float32).reshape(seqs, heads, per_group, hd), q_gain
    ).astype(jnp.bfloat16)
    query = query.transpose(1, 0, 2, 3).reshape(heads * seqs * per_group, hd)
    start = lax.axis_index("tp") * used
    query = lax.dynamic_slice_in_dim(query, start, used, 0)
    bias = jnp.broadcast_to(stick_bias.reshape(heads, 1, per_group, 1), (heads, seqs, per_group, hd))
    bias = lax.dynamic_slice_in_dim(bias.reshape(heads * seqs * per_group, hd), start, used, 0)
    if lines > used:
        query = jnp.pad(query, ((0, lines - used), (0, 0)))
        bias = jnp.pad(bias, ((0, lines - used), (0, 0)))
    span = ntp * tok_seq
    dma = pltpu.SemaphoreType.DMA
    anywhere = pl.BlockSpec(memory_space=pl.ANY)
    vmem = pl.BlockSpec(memory_space=pltpu.VMEM)
    cache = jax.ShapeDtypeStruct((group_rows, span, hd), jnp.bfloat16)
    key_cache, value_cache, read = pl.pallas_call(
        functools.partial(kernel, (nsp, ntp, heads, q, group_rows, per_group)),
        out_shape=(cache, cache, jax.ShapeDtypeStruct((lines, hd), jnp.float32)),
        in_specs=[anywhere, vmem, anywhere, anywhere, vmem, vmem, vmem],
        out_specs=(anywhere, anywhere, vmem),
        scratch_shapes=[
            pltpu.VMEM((seqs, tok_seq, width), jnp.bfloat16),
            pltpu.VMEM((seqs, tok_seq, width), jnp.bfloat16),
            pltpu.VMEM((heads, nz, CORES, rows, 2 * hd), jnp.bfloat16),
            pltpu.VMEM((heads, seqs, tok_seq, hd), jnp.bfloat16),
            pltpu.VMEM((heads, seqs, tok_seq, hd), jnp.bfloat16),
            pltpu.VMEM((group_rows, span, hd), jnp.bfloat16),
            pltpu.VMEM((group_rows, span, hd), jnp.bfloat16),
            pltpu.VMEM((nsp, lines, 2 * hd), jnp.float32),
            dma,
            dma((heads, 2)),
            dma((heads, nz)),
            dma((heads, nz)),
            dma((heads, q, nz)),
            dma((heads, q, nz)),
            dma((heads,)),
            dma((heads,)),
            dma((2, ntp)),
            dma((2, ntp)),
            dma((2,)),
            dma((2,)),
            dma((nsp,)),
            dma((nsp,)),
        ],
        compiler_params=pltpu.CompilerParams(
            collective_id=0, has_side_effects=True, vmem_limit_bytes=56 * 1024 * 1024
        ),
    )(tokens, in_gain.reshape(1, width), w_key, w_value, k_gain.reshape(1, hd), query, bias)
    return key_cache, value_cache, read[:used].reshape(group_rows, per_group * hd)


def solution(mesh):
    return jax.shard_map(
        functools.partial(shards, (mesh.shape["sp"], mesh.shape["tp"])),
        mesh=mesh,
        in_specs=(
            P(None, ("sp", "tp"), None),
            P(),
            P("tp", None),
            P("tp", None),
            P(),
            P(),
            P(),
            P(),
        ),
        out_specs=(P("tp", "sp", None), P("tp", "sp", None), P("tp", None)),
        check_vma=False,
    )
```

time: 153 us -> 72.6 us (0.47)
  the two profiles are of different devices: /device:TPU:0 before, /device:TPU:1 now
where the time goes in v1:
time: 72.6 us; the launch traced here: 72.2 us
  Pallas kernels  62.3 us (86%)
  local copies, waits for them, and re-layouts  7.59 us (10%)
  other arithmetic  1.62 us (2%)
    pallas_call x1, Pallas kernels, shards(): pl.pallas_call(functools.partial(kernel, (nsp, ntp, heads, q, group_rows,...  62.3 us
    unnamed x2, local copies, waits for them, and re-layouts  4.13 us
    broadcast_in_dim x4, local copies, waits for them, and re-layouts, shards(): jnp.broadcast_to(stick_bias.reshape(heads, 1, per_group, 1), (heads, seqs...  1.51 us

profile of v1, /device:TPU:1, one launch (start us, length us, event | category | flops | bytes accessed | tf_op | source)
XLA Modules:
  0.0 72.2 jit_solution(13712943433950968884)
XLA Ops:
  0.6 0.7 %broadcast_in_dim.13 = f32[4,2]{1,0:T(4,128)S(1)} reshape(f32[8]{0:T(128)} %param.15) | data formatting | bytes 64 | tf_op jit(solution)/shard_map/broadcast_in_dim | solution.py:273
  1.4 0.8 %fusion = f32[8,4,2]{0,2,1:T(2,128)S(1)} fusion(bf16[8,4,2,128]{3,0,2,1:T(8,128)(2,1)} %bitcast.7), kind=kLoop, calls=%fused_computation.2 | loop fusion | flops 24512 | bytes 16640 | tf_op jit(solution)/shard_map/reduce_sum | solution.py:17
  2.2 0.8 %fusion.3 = bf16[4,8,2,128]{3,1,2,0:T(8,128)(2,1)S(1)} fusion(bf16[8,4,2,128]{3,0,2,1:T(8,128)(2,1)} %bitcast.8, f32[128]{0:T(128)} %param.14, f32[8,4,2]{0,2,1:T(2,128)S(1)} %add_rsqrt_fusion), kind=kLoop, calls=%fused_computation.5 | loop fusion | flops 32768 | bytes 33536 | tf_op jit(solution)/shard_map/transpose | solution.py:270
  3.0 0.6 constant_dynamic-slice_fusion.query_ref
  3.6 0.1 broadcast_in_dim.15
  3.7 0.1 dynamic_slice.7
  3.8 0.7 broadcast_in_dim.16.bias_ref
  4.5 62.3 %shard_map.103 = (bf16[4,768,128]{2,1,0:T(8,128)(2,1)}, bf16[4,768,128]{2,1,0:T(8,128)(2,1)}, f32[8,128]{1,0:T(8,128)}) custom-call(bf16[8,96,2048]{2,1,0:T(8,128)(2,1)} %tok_hbm.1, f32[1,2048]{1,0:T(1,128)} %bitcast.10, bf16[256,512]{1,0:T(8,128)(2,1)} %wk_hbm.1, bf16[256,512]{1,0:T(8,128)(2,1)} %wv_hbm.1, f32[1,128]{1,0:T(1,128)} %bitcast.11, ...), custom_call_target="tpu_custom_call" | custom-call | tf_op jit(solution)/shard_map/pallas_call | solution.py:283
  66.8 1.3 %reshape.42 = f32[4,256]{1,0:T(4,128)} reshape(f32[8,128]{1,0:T(8,128)} %get-tuple-element.8) | data formatting | bytes 8192 | tf_op jit(solution)/shard_map/reshape | solution.py:316
  68.0 2.1 %copy.16 = bf16[4,768,128]{2,1,0:T(8,128)(2,1)} copy(bf16[4,768,128]{2,1,0:T(8,128)(2,1)} %get-tuple-element.12) | data formatting | bytes 1572864
  70.1 2.1 %copy.17 = bf16[4,768,128]{2,1,0:T(8,128)(2,1)} copy(bf16[4,768,128]{2,1,0:T(8,128)(2,1)} %get-tuple-element.13) | data formatting | bytes 1572864
  (3 shorter events, 0.0 us)

commit v2 on v1

v2 whole, which is shorter than its diff:
```python
import functools

import jax
import jax.numpy as jnp
from jax import lax
from jax.experimental import pallas as pl
from jax.experimental.pallas import tpu as pltpu
from jax.sharding import PartitionSpec as P

NORM_EPS = 1e-06
MESH = pl.DeviceIdType.MESH
CORES = 2
SUBLANES = 16


def root_norm(values, scaling):
    inverse = lax.rsqrt(jnp.mean(values * values, axis=-1, keepdims=True) + NORM_EPS)
    return values * inverse * scaling


def remote(src, dst, send, recv, sp, tp):
    return pltpu.make_async_remote_copy(
        src_ref=src, dst_ref=dst, send_sem=send, recv_sem=recv, device_id=(sp, tp), device_id_type=MESH
    )


def kernel(
    dims,
    tok_hbm, gain_ref, wk_hbm, wv_hbm, kgain_ref, query_ref, qgain_ref, bias_ref,
    krecv, vrecv, read_ref,
    tok, normed, wbuf, kvbuf, parts, qall, query,
    tok_sem, own_sem, p1_send, p1_recv, p2_send, p2_recv, p3_send, p3_recv,
    a_send, a_recv, mine_sem, f_send, f_recv,
):
    nsp, ntp, heads, q, group_rows, per_group = dims
    sp, tp = lax.axis_index("sp"), lax.axis_index("tp")
    nz = ntp // CORES
    z, c = tp // CORES, tp % CORES
    partner = z * CORES + (1 - c)
    base, i = (sp // q) * q, sp % q
    seqs, tok_seq, width = tok.shape
    rows = wk_hbm.shape[0]
    part = rows // q
    hd = krecv.shape[2]
    span = ntp * tok_seq
    tp_head = ntp // heads
    half = heads // 2

    def head_at(zc, j):
        home = (zc * CORES) // tp_head
        side = (home // half + (1 if j < half else 0)) % 2
        return side * half + (home % half + (half - 1 - j % half)) % half

    chunks = 2 * heads

    def chunk(zc, m):
        return m // heads, head_at(zc, m % heads)

    fetch = pltpu.make_async_copy(tok_hbm, tok, tok_sem)
    own = []
    for m in range(chunks):
        n, h = chunk(z, m)
        cols = pl.ds(pl.multiple_of(h * hd, hd), hd)
        copy = pltpu.make_async_copy(
            (wk_hbm, wv_hbm)[n].at[:, cols], wbuf.at[n, h, z, c], own_sem.at[m]
        )
        copy.start()
        own.append(copy)
    fetch.start()

    barrier = pltpu.get_barrier_semaphore()
    for d in range(1, ntp):
        pl.semaphore_signal(barrier, inc=1, device_id=(sp, (tp + d) % ntp), device_id_type=MESH)
    for d in range(1, nsp):
        pl.semaphore_signal(barrier, inc=1, device_id=((sp + d) % nsp, tp), device_id_type=MESH)
    for copy in own:
        copy.wait()
    pl.semaphore_wait(barrier, ntp + nsp - 2)

    mine = pl.ds(pl.multiple_of(i * part, part), part)
    sends = []

    for m in range(chunks):
        for d in range(1, nz):
            zt = (z + d) % nz
            n, h = chunk(zt, m)
            block = wbuf.at[n, h, z, c, mine]
            copy = remote(block, block, p1_send.at[m, d], p1_recv.at[m, z], sp, zt * CORES + c)
            copy.start()
            sends.append(copy)

    fetch.wait()
    step_rows = SUBLANES
    per_seq = tok_seq // step_rows

    def norm_rows(n, carry):
        s, at = n // per_seq, pl.ds(pl.multiple_of((n % per_seq) * step_rows, step_rows), step_rows)
        values = tok[s, at].astype(jnp.float32)
        normed[s, at] = root_norm(values, gain_ref[...]).astype(jnp.bfloat16)
        return carry

    lax.fori_loop(0, seqs * per_seq, norm_rows, 0)

    count = query_ref.shape[1] // hd
    for k in range(count):
        values = query_ref[:, k * hd : (k + 1) * hd].astype(jnp.float32)
        qall[k] = root_norm(values, qgain_ref[...])
    group = tp // tp_head
    start = (tp % tp_head) * group_rows
    lines = query.shape[0]
    query[...] = jnp.zeros_like(query)
    for r in range(group_rows):
        for k in range(per_group):
            query[pl.ds(r * per_group + k, 1)] = qall[group * per_group + k, pl.ds(start + r, 1)]
    lanes = lax.broadcasted_iota(jnp.int32, (lines, count), 1)
    which = group * per_group + lax.broadcasted_iota(jnp.int32, (lines, count), 0) % per_group
    bias = jnp.sum(jnp.where(lanes == which, bias_ref[...], 0.0), axis=1, keepdims=True)

    def spread(m):
        n, h = chunk(z, m)
        for d in range(1, nz):
            zs = (z + nz - d) % nz
            block = wbuf.at[n, h, zs, c, mine]
            remote(block, block, p1_send.at[m, d], p1_recv.at[m, zs], sp, zs * CORES + c).wait_recv()
            for e in range(1, q):
                copy = remote(
                    block, block, p2_send.at[m, e, d], p2_recv.at[m, i, zs], base + (i + e) % q, tp
                )
                copy.start()
                sends.append(copy)

    def share(m):
        n, h = chunk(z, m)
        for d in range(1, nz):
            zs = (z + nz - d) % nz
            for e in range(1, q):
                source = (i + e) % q
                block = wbuf.at[n, h, zs, c, pl.ds(pl.multiple_of(source * part, part), part)]
                remote(
                    block, block, p2_send.at[m, e, d], p2_recv.at[m, source, zs], base + source, tp
                ).wait_recv()
        block = wbuf.at[n, h, :, c]
        copy = remote(block, block, p3_send.at[m], p3_recv.at[m], sp, partner)
        copy.start()
        sends.append(copy)

    tile = seqs // 2

    def project(m):
        n, h = chunk(z, m)
        block = wbuf.at[n, h, :, 1 - c]
        remote(block, block, p3_send.at[m], p3_recv.at[m], sp, partner).wait_recv()

        def rows_of(k, carry):
            at = pl.ds(k * tile, tile)
            out = jnp.dot(
                normed[at].reshape(tile * tok_seq, width),
                wbuf[n, h].reshape(width, hd),
                preferred_element_type=jnp.float32,
            )
            if n == 0:
                out = root_norm(out, kgain_ref[...])
            kvbuf[n, h, at] = out.astype(jnp.bfloat16).reshape(tile, tok_seq, hd)
            return carry

        lax.fori_loop(0, seqs // tile, rows_of, 0)

    here = pl.ds(pl.multiple_of(tp * tok_seq, tok_seq), tok_seq)
    landing = (krecv, vrecv)

    def deliver(m):
        n, h = chunk(z, m)
        for u in range(tp_head):
            target = h * tp_head + u
            block = kvbuf.at[n, h, pl.ds(u * group_rows, group_rows)]
            copy = remote(
                block, landing[n].at[:, here], a_send.at[n, target], a_recv.at[n, tp], sp, target
            )
            if m % heads < heads - 1:
                copy.start()
            else:

                @pl.when(target != tp)
                def _(copy=copy):
                    copy.start()

                @pl.when(target == tp)
                def _(block=block):
                    pltpu.make_async_copy(block, landing[n].at[:, here], mine_sem.at[n]).start()

    first = pl.ds(0, group_rows)

    def arrived(n):
        block = kvbuf.at[n, 0, first]
        pltpu.make_async_copy(block, landing[n].at[:, here], mine_sem.at[n]).wait()
        for d in range(1, ntp):
            source = (tp + d) % ntp
            at = pl.ds(pl.multiple_of(source * tok_seq, tok_seq), tok_seq)
            remote(
                block, landing[n].at[:, at], a_send.at[n, source], a_recv.at[n, source], sp, source
            ).wait_recv()

    spread(0)
    for m in range(chunks):
        if m + 1 < chunks:
            spread(m + 1)
        share(m)
        project(m)
        deliver(m)
    arrived(0)

    line = lax.broadcasted_iota(jnp.int32, (lines, 1), 0) // per_group
    raw = jnp.zeros((lines, span), jnp.float32)
    for r in range(group_rows):
        dots = lax.dot_general(
            query[...].astype(jnp.bfloat16), krecv[r], (((1,), (1,)), ((), ())), preferred_element_type=jnp.float32
        )
        raw = jnp.where(line == r, dots, raw)
    scores = raw * hd ** (-0.5) + bias
    soft = jnp.log1p(jnp.exp(-jnp.abs(scores)))
    keep = -jnp.maximum(scores, 0.0) - soft
    take = jnp.minimum(scores, 0.0) - soft
    place = lax.broadcasted_iota(jnp.int32, (lines, span), 1)
    total = keep
    reach = 1
    while reach < span:
        moved = pltpu.roll(total, span - reach, 1)
        total = total + jnp.where(place < span - reach, moved, 0.0)
        reach *= 2
    weights = jnp.exp(take + (total - keep)).astype(jnp.bfloat16)
    arrived(1)
    value = jnp.zeros((lines, hd), jnp.float32)
    for r in range(group_rows):
        dots = jnp.dot(weights, vrecv[r], preferred_element_type=jnp.float32)
        value = jnp.where(line == r, dots, value)
    parts[sp, :, :hd] = value
    parts[sp, :, hd:] = jnp.broadcast_to(total[:, :1], (lines, hd))
    for d in range(1, nsp):
        copy = remote(
            parts.at[sp], parts.at[sp], f_send.at[d], f_recv.at[sp], (sp + d) % nsp, tp
        )
        copy.start()
        sends.append(copy)
    for d in range(1, nsp):
        source = (sp + d) % nsp
        remote(parts.at[source], parts.at[source], f_send.at[d], f_recv.at[source], source, tp).wait_recv()
    result = jnp.zeros((lines, hd), jnp.float32)
    later = jnp.zeros((lines, hd), jnp.float32)
    for n in reversed(range(nsp)):
        result = result + jnp.exp(later) * parts[n, :, :hd]
        later = later + parts[n, :, hd:]
    for r in range(group_rows):
        for k in range(per_group):
            at = r * per_group + k
            read_ref[r : r + 1, k * hd : (k + 1) * hd] = result[at : at + 1]

    for copy in sends:
        copy.wait_send()
    for d in range(1, ntp):
        target = (tp + d) % ntp
        for n in range(2):
            remote(
                kvbuf.at[n, 0, first], landing[n].at[:, here], a_send.at[n, target], a_recv.at[n, tp], sp, target
            ).wait_send()


def shards(sizes, tokens, in_gain, w_key, w_value, k_gain, new_query, q_gain, stick_bias):
    nsp, ntp = sizes
    seqs, tok_seq, width = tokens.shape
    rows, kv_width = w_key.shape
    hd = k_gain.shape[0]
    heads = kv_width // hd
    per_group = stick_bias.shape[0] // heads
    group_rows = heads * seqs // ntp
    used = group_rows * per_group
    lines = -(-used // 8) * 8
    nz = ntp // CORES
    q = min(nsp, rows // SUBLANES)
    span = ntp * tok_seq
    dma = pltpu.SemaphoreType.DMA
    hbm = pl.BlockSpec(memory_space=pltpu.HBM)
    vmem = pl.BlockSpec(memory_space=pltpu.VMEM)
    cache = ((group_rows, span, hd), jnp.bfloat16)
    read = ((group_rows, per_group * hd), jnp.float32)
    chunks = 2 * heads
    return pl.pallas_call(
        functools.partial(kernel, (nsp, ntp, heads, q, group_rows, per_group)),
        out_shape=(pltpu.VMEM(*cache), pltpu.VMEM(*cache), pltpu.VMEM(*read)),
        in_specs=[hbm, vmem, hbm, hbm, vmem, vmem, vmem, vmem],
        out_specs=(vmem, vmem, vmem),
        scratch_shapes=[
            pltpu.VMEM((seqs, tok_seq, width), jnp.bfloat16),
            pltpu.VMEM((seqs, tok_seq, width), jnp.bfloat16),
            pltpu.VMEM((2, heads, nz, CORES, rows, hd), jnp.bfloat16),
            pltpu.VMEM((2, heads, seqs, tok_seq, hd), jnp.bfloat16),
            pltpu.VMEM((nsp, lines, 2 * hd), jnp.float32),
            pltpu.VMEM((heads * per_group, seqs, hd), jnp.float32),
            pltpu.VMEM((lines, hd), jnp.float32),
            dma,
            dma((chunks,)),
            dma((chunks, nz)),
            dma((chunks, nz)),
            dma((chunks, q, nz)),
            dma((chunks, q, nz)),
            dma((chunks,)),
            dma((chunks,)),
            dma((2, ntp)),
            dma((2, ntp)),
            dma((2,)),
            dma((nsp,)),
            dma((nsp,)),
        ],
        compiler_params=pltpu.CompilerParams(
            collective_id=0, has_side_effects=True, vmem_limit_bytes=62 * 1024 * 1024
        ),
    )(
        tokens,
        in_gain.reshape(1, width),
        w_key,
        w_value,
        k_gain.reshape(1, hd),
        new_query,
        q_gain.reshape(1, hd),
        stick_bias.reshape(1, heads * per_group),
    )

def solution(mesh):
    return jax.shard_map(
        functools.partial(shards, (mesh.shape["sp"], mesh.shape["tp"])),
        mesh=mesh,
        in_specs=(
            P(None, ("sp", "tp"), None),
            P(),
            P("tp", None),
            P("tp", None),
            P(),
            P(),
            P(),
            P(),
        ),
        out_specs=(P("tp", "sp", None), P("tp", "sp", None), P("tp", None)),
        check_vma=False,
    )
```

time: 72.6 us -> 63.9 us (0.88)
  the two profiles are of different devices: /device:TPU:1 before, /device:TPU:0 now
where the time goes in v2:
time: 63.9 us; the launch traced here: 63.8 us
  Pallas kernels  60.8 us (95%)
  local copies, waits for them, and re-layouts  2.35 us (4%)
  between operations  0.64 us (1%)
    pallas_call x1, Pallas kernels, shards(): pl.pallas_call(functools.partial(kernel, (nsp, ntp, heads, q, group_rows,...  60.8 us
    unnamed x3, local copies, waits for them, and re-layouts  2.35 us

profile of v2, /device:TPU:0, one launch (start us, length us, event | category | flops | bytes accessed | tf_op | source)
XLA Modules:
  0.0 63.8 jit_solution(17677611693872304767)
XLA Ops:
  0.6 60.8 %shard_map.103 = (bf16[4,768,128]{2,1,0:T(8,128)(2,1)S(1)}, bf16[4,768,128]{2,1,0:T(8,128)(2,1)S(1)}, f32[4,256]{1,0:T(4,128)S(1)}) custom-call(bf16[8,96,2048]{2,1,0:T(8,128)(2,1)} %tok_hbm.1, f32[1,2048]{1,0:T(1,128)} %bitcast.4, bf16[256,512]{1,0:T(8,128)(2,1)} %wk_hbm.1, bf16[256,512]{1,0:T(8,128)(2,1)} %wv_hbm.1, f32[1,128]{1,0:T(1,128)} %bitcast.5, ...), custom_call_target="tpu_custom_call" | custom-call | tf_op jit(solution)/shard_map/pallas_call | solution.py:286
  61.4 0.9 %copy.14 = bf16[4,768,128]{2,1,0:T(8,128)(2,1)} copy(bf16[4,768,128]{2,1,0:T(8,128)(2,1)S(1)} %get-tuple-element.3) | data formatting | bytes 1572864
  62.3 0.6 copy.16
  62.9 0.9 %copy.15 = bf16[4,768,128]{2,1,0:T(8,128)(2,1)} copy(bf16[4,768,128]{2,1,0:T(8,128)(2,1)S(1)} %get-tuple-element.4) | data formatting | bytes 1572864

commit v3 on v2

--- a/solution.py
+++ b/solution.py
@@ -73,14 +73,15 @@
         pl.semaphore_signal(barrier, inc=1, device_id=(sp, (tp + d) % ntp), device_id_type=MESH)
     for d in range(1, nsp):
         pl.semaphore_signal(barrier, inc=1, device_id=((sp + d) % nsp, tp), device_id_type=MESH)
-    for copy in own:
-        copy.wait()
     pl.semaphore_wait(barrier, ntp + nsp - 2)
 
     mine = pl.ds(pl.multiple_of(i * part, part), part)
     sends = []
 
     for m in range(chunks):
+        if m % heads == 0:
+            for copy in own[m : m + heads]:
+                copy.wait()
         for d in range(1, nz):
             zt = (z + d) % nz
             n, h = chunk(zt, m)
@@ -96,10 +97,14 @@
     def norm_rows(n, carry):
         s, at = n // per_seq, pl.ds(pl.multiple_of((n % per_seq) * step_rows, step_rows), step_rows)
         values = tok[s, at].astype(jnp.float32)
-        normed[s, at] = root_norm(values, gain_ref[...]).astype(jnp.bfloat16)
+        inverse = lax.rsqrt(jnp.mean(values * values, axis=-1, keepdims=True) + NORM_EPS)
+        values = tok[s, at].astype(jnp.float32)
+        normed[s, at] = (values * inverse * gain_ref[...]).astype(jnp.bfloat16)
         return carry
 
-    lax.fori_loop(0, seqs * per_seq, norm_rows, 0)
+    def norm_share(n, shares):
+        steps = seqs * per_seq
+        lax.fori_loop(steps * n // shares, steps * (n + 1) // shares, norm_rows, 0, unroll=4)
 
     count = query_ref.shape[1] // hd
     for k in range(count):
@@ -144,14 +149,14 @@
         copy.start()
         sends.append(copy)
 
-    tile = seqs // 2
+    tile = max(seqs // 2, group_rows)
 
     def project(m):
         n, h = chunk(z, m)
         block = wbuf.at[n, h, :, 1 - c]
         remote(block, block, p3_send.at[m], p3_recv.at[m], sp, partner).wait_recv()
 
-        def rows_of(k, carry):
+        for k in range(seqs // tile):
             at = pl.ds(k * tile, tile)
             out = jnp.dot(
                 normed[at].reshape(tile * tok_seq, width),
@@ -161,16 +166,15 @@
             if n == 0:
                 out = root_norm(out, kgain_ref[...])
             kvbuf[n, h, at] = out.astype(jnp.bfloat16).reshape(tile, tok_seq, hd)
-            return carry
-
-        lax.fori_loop(0, seqs // tile, rows_of, 0)
+            per_tile = tile // group_rows
+            deliver(m, range(k * per_tile, (k + 1) * per_tile))
 
     here = pl.ds(pl.multiple_of(tp * tok_seq, tok_seq), tok_seq)
     landing = (krecv, vrecv)
 
-    def deliver(m):
-        n, h = chunk(z, m)
-        for u in range(tp_head):
+    def deliver(m, pieces):
+        n, h = chunk(z, m)
+        for u in pieces:
             target = h * tp_head + u
             block = kvbuf.at[n, h, pl.ds(u * group_rows, group_rows)]
             copy = remote(
@@ -200,13 +204,16 @@
                 block, landing[n].at[:, at], a_send.at[n, source], a_recv.at[n, source], sp, source
             ).wait_recv()
 
+    norm_share(0, 3)
     spread(0)
+    norm_share(1, 3)
     for m in range(chunks):
         if m + 1 < chunks:
             spread(m + 1)
         share(m)
+        if m == 0:
+            norm_share(2, 3)
         project(m)
-        deliver(m)
     arrived(0)
 
     line = lax.broadcasted_iota(jnp.int32, (lines, 1), 0) // per_group
@@ -324,6 +331,7 @@
         stick_bias.reshape(1, heads * per_group),
     )
 
+
 def solution(mesh):
     return jax.shard_map(
         functools.partial(shards, (mesh.shape["sp"], mesh.shape["tp"])),

time: 63.9 us -> 62.2 us (0.973)
  Pallas kernels: 60.8 us -> 59 us
    pallas_call x1, Pallas kernels: 60.8 us -> 59 us  [shards(): pl.pallas_call(functools.partial(kernel, (nsp, ntp, heads, q, group_rows,...]
where the time goes in v3:
time: 62.2 us; the launch traced here: 62 us
  Pallas kernels  59 us (95%)
  local copies, waits for them, and re-layouts  2.35 us (4%)
  between operations  0.64 us (1%)
    pallas_call x1, Pallas kernels, shards(): pl.pallas_call(functools.partial(kernel, (nsp, ntp, heads, q, group_rows,...  59 us
    unnamed x3, local copies, waits for them, and re-layouts  2.35 us

profile of v3, /device:TPU:0, one launch (start us, length us, event | category | flops | bytes accessed | tf_op | source)
XLA Modules:
  0.0 62.0 jit_solution(10568859864042875801)
XLA Ops:
  0.6 59.0 %shard_map.103 = (bf16[4,768,128]{2,1,0:T(8,128)(2,1)S(1)}, bf16[4,768,128]{2,1,0:T(8,128)(2,1)S(1)}, f32[4,256]{1,0:T(4,128)S(1)}) custom-call(bf16[8,96,2048]{2,1,0:T(8,128)(2,1)} %tok_hbm.1, f32[1,2048]{1,0:T(1,128)} %bitcast.4, bf16[256,512]{1,0:T(8,128)(2,1)} %wk_hbm.1, bf16[256,512]{1,0:T(8,128)(2,1)} %wv_hbm.1, f32[1,128]{1,0:T(1,128)} %bitcast.5, ...), custom_call_target="tpu_custom_call" | custom-call | tf_op jit(solution)/shard_map/pallas_call | solution.py:293
  59.7 0.9 %copy.14 = bf16[4,768,128]{2,1,0:T(8,128)(2,1)} copy(bf16[4,768,128]{2,1,0:T(8,128)(2,1)S(1)} %get-tuple-element.3) | data formatting | bytes 1572864
  60.6 0.6 copy.16
  61.2 0.9 %copy.15 = bf16[4,768,128]{2,1,0:T(8,128)(2,1)} copy(bf16[4,768,128]{2,1,0:T(8,128)(2,1)S(1)} %get-tuple-element.4) | data formatting | bytes 1572864
